TPU v7x, 32 devices: a whole 2x2x4 slice. The times are simulated.
32 devices in a mesh: grp: 2 (over y), sp: 4 (over z), tp: 4 (over x, core).
Axes of the slice: x: 2, y: 2, z: 4, core: 2. Of those that a mesh axis runs over, the one named last changes fastest.
Arguments:
- input_wide: bfloat16 [1024, 512], P(('grp', 'sp'), 'tp'), parts along dimension 0, may hold values from -6 to 6
- input_narrow: bfloat16 [1024, 512], P(('grp', 'sp'), 'tp'), parts along dimension 0, may hold values from -6 to 6
- spacing: float32 [1024], P(('grp', 'sp')), parts along dimension 0, may hold values from 0.2 to 208
- rate_wide: float32 [2, 32, 64], P(None, 'tp'), may hold values from 0.0009765625 to 0.035
- turn_wide: float32 [2, 32, 64], P(None, 'tp'), may hold values from 0.1 to 1.5
- drive_wide: float32 [2, 32, 16, 128], P(None, 'tp'), may hold values from -0.2 to 0.2
- read_wide: float32 [2, 32, 16, 128], P(None, 'tp'), may hold values from -0.5 to 0.5
- narrow_decay_rate: float32 [2, 32, 32], P(None, 'tp'), may hold values from 0.0009765625 to 0.035
- turn_narrow: float32 [2, 32, 32], P(None, 'tp'), may hold values from 0.1 to 1.5
- drive_narrow: float32 [2, 32, 16, 64], P(None, 'tp'), may hold values from -0.2 to 0.2
- read_narrow: float32 [2, 32, 16, 64], P(None, 'tp'), may hold values from -0.75 to 0.75
- skip_gain: float32 [2, 512], P(None, 'tp'), may hold values from -4 to 4
- out_value: bfloat16 [1024, 1024], P(None, 'tp'), may hold values from -0.1875 to 0.1875
- out_gate: bfloat16 [1024, 1024], P(None, 'tp'), may hold values from -0.1875 to 0.1875
- stream: bfloat16 [1024, 1024], P(('grp', 'sp'), 'tp'), parts along dimension 0, may hold values from -20 to 20
- norm_gain: float32 [1024], P('tp'), may hold values from 0.1 to 1.9
- up_value: bfloat16 [1024, 5632], P('sp', 'tp'), may hold values from -0.1875 to 0.1875
- up_gate: bfloat16 [1024, 5632], P('sp', 'tp'), may hold values from -0.1875 to 0.1875
- conv_taps: float32 [2, 3, 5632], P(None, None, 'tp'), may hold values from -3.5 to 3.5
- down_weight: bfloat16 [5632, 1024], P('tp', 'sp'), may hold values from -0.078125 to 0.078125
Outputs:
- mixed: bfloat16 [1024, 1024], P(('grp', 'sp'), 'tp'), parts along dimension 0
There are 2 independent parts, one for each index of `grp`. A program takes and returns all parts, laid end to end along the dimension named above; an argument that names none is the same for every part. Nothing has to cross between parts.
All inputs are finite; a program needn't handle non-finite values.
Results may differ from a plain program's by a relative error of at most 0.017.
Values may be sent and summed in bfloat16 or wider, within the bound.
A program may use at most 128 MiB of HBM per device.

v0:
```python
import jax
import jax.numpy as jnp
from jax import lax
from jax.sharding import PartitionSpec as P

DA = 512
GROUP = 16
D = 1024


precise = lax.Precision.HIGHEST
epsilon = 1e-06


def extended(block, sides, width):
    for axis, dim in sides:
        count = lax.axis_size(axis)
        forward = [(i, i + 1) for i in range(count - 1)]
        backward = [(target, source) for source, target in forward]
        low = lax.ppermute(
            lax.slice_in_dim(block, block.shape[dim] - width, None, axis=dim), axis, forward
        )
        high = lax.ppermute(lax.slice_in_dim(block, 0, width, axis=dim), axis, backward)
        block = jnp.concatenate([low, block, high], axis=dim)
    return block


def complex_times(left_real, left_quad, right_real, right_quad):
    return (
        left_real * right_real - left_quad * right_quad,
        left_real * right_quad + left_quad * right_real,
    )


def step_factors(rate, turn, spacing):
    shrink = jnp.exp(-rate * spacing)
    angle = turn * spacing
    decay_real = shrink * jnp.cos(angle)
    decay_quad = shrink * jnp.sin(angle)
    square = rate * rate + turn * turn
    coef_real, coef_quad = complex_times(
        decay_real - 1.0, decay_quad, -rate / square, -turn / square
    )
    return (decay_real, decay_quad, coef_real, coef_quad)


def turned(rate, turn, span, state_real, state_quad):
    shrink = jnp.exp(-rate * span)
    angle = turn * span
    return complex_times(shrink * jnp.cos(angle), shrink * jnp.sin(angle), state_real, state_quad)


def pair_combine(early, later):
    decay_real, decay_quad = complex_times(early[0], early[1], later[0], later[1])
    shifted_real, moved_quad = complex_times(later[0], later[1], early[2], early[3])
    return (decay_real, decay_quad, shifted_real + later[2], moved_quad + later[3])


def block_pass(clustered, spacing, rate_flat, turn_flat, drive, reverse):
    extent = clustered.shape[0]
    states = drive.shape[2] // 2
    decay_real, decay_quad, coef_real, coef_quad = step_factors(
        rate_flat, turn_flat, spacing[:, None]
    )
    pushed = jnp.einsum("tgc,gcq->tgq", clustered, drive, precision=precise)
    push_real = pushed[..., :states].reshape(extent, -1)
    push_quad = pushed[..., states:].reshape(extent, -1)
    kick_real, impulse_quadrature = complex_times(coef_real, coef_quad, push_real, push_quad)
    scanned = lax.associative_scan(
        pair_combine,
        (decay_real, decay_quad, kick_real, impulse_quadrature),
        reverse=reverse,
        axis=0,
    )
    return (scanned[2], scanned[3])


def on_device(
    input_wide,
    input_narrow,
    spacing,
    rate_wide,
    turn_wide,
    drive_wide,
    read_wide,
    narrow_decay_rate,
    turn_narrow,
    drive_narrow,
    read_narrow,
    skip_gain,
    out_value,
    out_gate,
    stream,
    norm_gain,
    up_value,
    up_gate,
    conv_taps,
    down_weight,
):
    extent = input_wide.shape[0]
    sets = (
        (input_wide, rate_wide.reshape(2, -1), turn_wide.reshape(2, -1), drive_wide, read_wide),
        (
            input_narrow,
            narrow_decay_rate.reshape(2, -1),
            turn_narrow.reshape(2, -1),
            drive_narrow,
            read_narrow,
        ),
    )
    passes = []
    for which in range(2):
        inputs, rate, turn, drive, read = sets[which]
        clustered = inputs.astype(jnp.float32).reshape(extent, drive.shape[1], GROUP)
        passes.append(
            (
                block_pass(clustered, spacing, rate[0], turn[0], drive[0], False),
                block_pass(clustered, spacing, rate[1], turn[1], drive[1], True),
            )
        )
    total = jnp.sum(spacing)
    ahead = jnp.cumsum(spacing)
    behind = total - ahead + spacing
    forward_ends = (
        total,
        passes[0][0][0][-1],
        passes[0][0][1][-1],
        passes[1][0][0][-1],
        passes[1][0][1][-1],
    )
    backward_ends = (
        total,
        passes[0][1][0][0],
        passes[0][1][1][0],
        passes[1][1][0][0],
        passes[1][1][1][0],
    )
    collected = lax.all_gather(
        tuple((item[None] for item in forward_ends + backward_ends[1:])), "sp", axis=0, tiled=True
    )
    count = lax.axis_size("sp")
    own_index = lax.axis_index("sp")
    order = jnp.arange(count)
    aggregates = collected[0]
    through = jnp.cumsum(aggregates)
    before = through[own_index] - aggregates[own_index]
    early_mask = order < own_index
    late_mask = order > own_index
    early_span = jnp.where(early_mask, before - through, 0.0)[:, None]
    late_span = jnp.where(late_mask, through - aggregates - through[own_index], 0.0)[:, None]
    carries = [[], []]
    for which in range(2):
        rate, turn = (sets[which][1], sets[which][2])
        part_real, part_quad = turned(
            rate[0], turn[0], early_span, collected[1 + 2 * which], collected[2 + 2 * which]
        )
        keep = early_mask[:, None]
        carries[0].append(
            (
                jnp.sum(jnp.where(keep, part_real, 0.0), axis=0),
                jnp.sum(jnp.where(keep, part_quad, 0.0), axis=0),
            )
        )
        part_real, part_quad = turned(
            rate[1], turn[1], late_span, collected[5 + 2 * which], collected[6 + 2 * which]
        )
        keep = late_mask[:, None]
        carries[1].append(
            (
                jnp.sum(jnp.where(keep, part_real, 0.0), axis=0),
                jnp.sum(jnp.where(keep, part_quad, 0.0), axis=0),
            )
        )
    mixer_parts = []
    for which in range(2):
        inputs, rate, turn, drive, read = sets[which]
        groups = drive.shape[1]
        states = drive.shape[3] // 2
        reading = jnp.zeros((extent, groups, GROUP), jnp.float32)
        for direction in range(2):
            local_real, local_imaginary = passes[which][direction]
            span = ahead if direction == 0 else behind
            carry_real, carry_quad = carries[direction][which]
            extra_real, extra_quad = turned(
                rate[direction], turn[direction], span[:, None], carry_real, carry_quad
            )
            joined = jnp.concatenate(
                [
                    (local_real + extra_real).reshape(extent, groups, states),
                    (local_imaginary + extra_quad).reshape(extent, groups, states),
                ],
                axis=2,
            )
            reading = reading + jnp.einsum(
                "tgq,gcq->tgc", joined, read[direction], precision=precise
            )
        reading = reading.reshape(extent, -1)
        mixer_parts.append(
            jax.nn.gelu(reading + skip_gain[which] * inputs.astype(jnp.float32)).astype(
                jnp.bfloat16
            )
        )
    pieces = (
        lax.all_gather(mixer_parts[0], "tp", axis=1, tiled=True),
        lax.all_gather(mixer_parts[1], "tp", axis=1, tiled=True),
    )
    count = pieces[0].shape[1]
    value_total = jnp.dot(
        pieces[0], lax.slice_in_dim(out_value, 0, count, axis=0), preferred_element_type=jnp.float32
    )
    value_total = value_total + jnp.dot(
        pieces[1],
        lax.dynamic_slice_in_dim(out_value, DA, count, 0),
        preferred_element_type=jnp.float32,
    )
    gate_total = jnp.dot(
        pieces[0], lax.slice_in_dim(out_gate, 0, count, axis=0), preferred_element_type=jnp.float32
    )
    gate_total = gate_total + jnp.dot(
        pieces[1],
        lax.dynamic_slice_in_dim(out_gate, DA, count, 0),
        preferred_element_type=jnp.float32,
    )
    middle = (stream.astype(jnp.float32) + value_total * jax.nn.sigmoid(gate_total)).astype(
        jnp.bfloat16
    )
    expanded_width = middle.astype(jnp.float32)
    squares = lax.psum(jnp.sum(expanded_width * expanded_width, axis=1), "tp")
    normed = (expanded_width * lax.rsqrt(squares / D + epsilon)[:, None] * norm_gain).astype(
        jnp.bfloat16
    )
    rows_whole = lax.all_gather(normed, "tp", axis=1, tiled=True)
    hidden_width = up_value.shape[1]
    whole_value, whole_gate = (
        lax.all_gather(up_value, "sp", axis=0, tiled=True),
        lax.all_gather(up_gate, "sp", axis=0, tiled=True),
    )
    value_pre = jnp.dot(rows_whole, whole_value, preferred_element_type=jnp.float32)
    gate_pre = jnp.dot(rows_whole, whole_gate, preferred_element_type=jnp.float32)
    pre = jnp.concatenate([value_pre, gate_pre], axis=1).astype(jnp.bfloat16)
    padded = extended(pre, (("sp", 0),), 1)
    taps = jnp.concatenate([conv_taps[0], conv_taps[1]], axis=1)
    conv = taps[0] * padded[:-2] + taps[1] * padded[1:-1] + taps[2] * padded[2:]
    hidden = (jax.nn.silu(conv[:, hidden_width:]) * conv[:, :hidden_width]).astype(jnp.bfloat16)
    down_whole = lax.all_gather(down_weight, "sp", axis=1, tiled=True)
    terms = jnp.dot(hidden, down_whole, preferred_element_type=jnp.float32)
    ffn = lax.psum_scatter(
        terms.astype(jnp.bfloat16), "tp", scatter_dimension=1, tiled=True
    ).astype(jnp.float32)
    return (middle.astype(jnp.float32) + ffn).astype(jnp.bfloat16)


def solution(mesh):
    placed = (
        P(("grp", "sp"), "tp"),
        P(("grp", "sp"), "tp"),
        P(("grp", "sp")),
        P(None, "tp", None),
        P(None, "tp", None),
        P(None, "tp", None, None),
        P(None, "tp", None, None),
        P(None, "tp", None),
        P(None, "tp", None),
        P(None, "tp", None, None),
        P(None, "tp", None, None),
        P(None, "tp"),
        P(None, "tp"),
        P(None, "tp"),
        P(("grp", "sp"), "tp"),
        P("tp"),
        P("sp", "tp"),
        P("sp", "tp"),
        P(None, None, "tp"),
        P("tp", "sp"),
    )
    return jax.shard_map(
        on_device, mesh=mesh, in_specs=placed, out_specs=P(("grp", "sp"), "tp"), check_vma=False
    )
```

profile of v0, /device:TPU:0, one launch (start us, length us, event | category | flops | bytes accessed | tf_op | source)
XLA Modules:
  0.0 850.6 jit_solution(5940520691749698102)
XLA Ops:
  45.1 6.4 slice.1639
  57.6 6.4 slice.1643
  64.0 6.4 slice.1656
  70.4 6.0 slice.1637
  76.5 6.4 slice.1648
  82.9 6.0 slice.1641
  89.0 6.4 slice.1650
  247.7 6.5 slice.1743
  254.3 6.5 slice.1747
  260.8 7.3 slice.1635
  268.1 6.5 slice.1738
  357.8 6.4 slice.1530
  370.3 6.4 slice.1538
  376.8 6.4 slice.1526
  383.2 6.3 slice.1532
  389.5 6.4 slice.1528
  395.9 6.6 slice.1533
  543.8 6.8 slice.1623
  550.6 6.8 slice.1626
  557.4 6.8 slice.1525
  564.3 6.8 slice.1619
  571.3 13.0 %all-gather.6 = f32[4,1,256]{2,1,0:T(1,128)S(1)} all-gather(f32[1,1,256]{2,1,0:T(1,128)} %add_bitcast_fusion.1), channel_id=1, replica_groups=mesh['grp'=2,'sp'=4,'tp'=4] {'sp'}, dimensions={0}, use_global_device_ids=true | all-gather | bytes 5120 | tf_op jit(solution)/shard_map/all_gather | solution.py:138
  584.3 7.9 all-gather.7
  594.7 10.3 %all-reduce.112 = f32[4]{0:T(128)S(1)} all-reduce(f32[4]{0:T(128)S(1)} %dynamic-update-slice), channel_id=1, replica_groups=mesh['grp'=2,'sp'=4,'tp'=4] {'sp'}, use_global_device_ids=true, to_apply=%add.112 | all-reduce | flops 4 | bytes 32
  622.4 7.7 all-gather.4
  630.2 9.7 %all-gather.5 = f32[4,1,256]{2,1,0:T(1,128)S(1)} all-gather(f32[1,1,256]{2,1,0:T(1,128)S(1)} %add_bitcast_fusion.2), channel_id=1, replica_groups=mesh['grp'=2,'sp'=4,'tp'=4] {'sp'}, dimensions={0}, use_global_device_ids=true | all-gather | bytes 5120 | tf_op jit(solution)/shard_map/all_gather | solution.py:138
  656.6 11.9 %all-gather.2 = f32[4,1,512]{2,1,0:T(1,128)S(1)} all-gather(f32[1,1,512]{2,1,0:T(1,128)S(1)} %bitcast.271), channel_id=1, replica_groups=mesh['grp'=2,'sp'=4,'tp'=4] {'sp'}, dimensions={0}, use_global_device_ids=true | all-gather | bytes 10240 | tf_op jit(solution)/shard_map/all_gather | solution.py:138
  668.5 11.9 %all-gather.3 = f32[4,1,512]{2,1,0:T(1,128)S(1)} all-gather(f32[1,1,512]{2,1,0:T(1,128)S(1)} %bitcast.270), channel_id=1, replica_groups=mesh['grp'=2,'sp'=4,'tp'=4] {'sp'}, dimensions={0}, use_global_device_ids=true | all-gather | bytes 10240 | tf_op jit(solution)/shard_map/all_gather | solution.py:138
  749.8 12.1 %all-gather = f32[4,1,512]{2,1,0:T(1,128)S(1)} all-gather(f32[1,1,512]{2,1,0:T(1,128)S(1)} %bitcast.272), channel_id=1, replica_groups=mesh['grp'=2,'sp'=4,'tp'=4] {'sp'}, dimensions={0}, use_global_device_ids=true | all-gather | bytes 10240 | tf_op jit(solution)/shard_map/all_gather | solution.py:138
  771.1 11.9 %all-gather.1 = f32[4,1,512]{2,1,0:T(1,128)S(1)} all-gather(f32[1,1,512]{2,1,0:T(1,128)S(1)} %bitcast.273), channel_id=1, replica_groups=mesh['grp'=2,'sp'=4,'tp'=4] {'sp'}, dimensions={0}, use_global_device_ids=true | all-gather | bytes 10240 | tf_op jit(solution)/shard_map/all_gather | solution.py:138
  794.3 7.1 psum.7
  823.2 18.9 %reduce-scatter.2.cloned.1.call-done = bf16[128,256]{1,0:T(8,128)(2,1)} async-done(((bf16[128,1024]{1,0:T(8,128)(2,1)}), bf16[128,256]{1,0:T(8,128)(2,1)}) %reduce-scatter.2.cloned.1.call-update) | async-done | bytes 65552 | tf_op jit(solution)/shard_map/reduce_scatter | solution.py:247
  (1050 shorter events, 572.5 us)
Async XLA Ops:
  6.5 801.1 %all-gather.14.cloned.1.call-start = ((), (), s32[]{:S(2)}) async-start(), calls=%async_computation.2 | async-start | bytes 3604480 | tf_op jit(solution)/shard_map/all_gather | solution.py:236
  7.3 802.8 %all-gather.12.cloned.1.call-start = ((), (), s32[]{:S(2)}) async-start(), calls=%async_computation.1 | async-start | bytes 3604480 | tf_op jit(solution)/shard_map/all_gather | solution.py:235
  8.0 812.0 %all-gather.16.cloned.1.call-start = ((), (), s32[]{:S(2)}) async-start(), calls=%async_computation.3 | async-start | bytes 3604480 | tf_op jit(solution)/shard_map/all_gather | solution.py:245
  8.8 833.4 %reduce-scatter.2.cloned.1.call-start = ((), (), s32[]{:S(2)}) async-start(), calls=%async_computation.4 | async-start | bytes 327680 | tf_op jit(solution)/shard_map/reduce_scatter | solution.py:247
  45.0 37.9 %copy-start = (f32[128,512]{0,1:T(8,128)}, f32[128,512]{0,1:T(8,128)S(1)}, u32[]{:S(2)}) copy-start(f32[128,512]{0,1:T(8,128)S(1)} %get-tuple-element.87) | copy-start | bytes 786436
  45.0 37.9 %copy-start.37 = (f32[128,512]{0,1:T(8,128)}, f32[128,512]{0,1:T(8,128)S(1)}, u32[]{:S(2)}) copy-start(f32[128,512]{0,1:T(8,128)S(1)} %get-tuple-element.283) | copy-start | bytes 786436
  45.1 43.9 %copy-start.35 = (f32[128,512]{0,1:T(8,128)}, f32[128,512]{0,1:T(8,128)S(1)}, u32[]{:S(2)}) copy-start(f32[128,512]{0,1:T(8,128)S(1)} %get-tuple-element.282) | copy-start | bytes 786436
  357.8 31.7 %copy-start.31 = (f32[128,512]{0,1:T(8,128)S(1)}, f32[128,512]{0,1:T(8,128)}, u32[]{:S(2)}) copy-start(f32[128,512]{0,1:T(8,128)} %get-tuple-element.317) | copy-start | bytes 786436
  540.1 31.0 %copy-start.93 = (f32[128,256]{1,0:T(8,128)S(1)}, f32[128,256]{1,0:T(8,128)}, u32[]{:S(2)}) copy-start(f32[128,256]{1,0:T(8,128)} %add.1387) | copy-start | bytes 393220
  564.3 51.2 %copy-start.137 = (f32[2,256]{1,0:T(2,128)S(1)}, f32[2,256]{1,0:T(2,128)}, u32[]{:S(2)}) copy-start(f32[2,256]{1,0:T(2,128)} %pad_add_fusion.6) | copy-start | bytes 6148
  564.3 52.0 %copy-start.138 = (f32[2,256]{1,0:T(2,128)S(1)}, f32[2,256]{1,0:T(2,128)}, u32[]{:S(2)}) copy-start(f32[2,256]{1,0:T(2,128)} %pad_add_fusion.7) | copy-start | bytes 6148
  564.3 52.0 %copy-start.127 = (f32[3,256]{1,0:T(4,128)S(1)}, f32[3,256]{1,0:T(4,128)}, u32[]{:S(2)}) copy-start(f32[3,256]{1,0:T(4,128)} %slice.1798) | copy-start | bytes 9220
  564.3 52.0 %copy-start.128 = (f32[3,256]{1,0:T(4,128)S(1)}, f32[3,256]{1,0:T(4,128)}, u32[]{:S(2)}) copy-start(f32[3,256]{1,0:T(4,128)} %slice.1829) | copy-start | bytes 9220
  564.3 52.0 %copy-start.129 = (f32[3,256]{1,0:T(4,128)S(1)}, f32[3,256]{1,0:T(4,128)}, u32[]{:S(2)}) copy-start(f32[3,256]{1,0:T(4,128)} %slice.1833) | copy-start | bytes 9220
  564.3 52.0 %copy-start.130 = (f32[3,256]{1,0:T(4,128)S(1)}, f32[3,256]{1,0:T(4,128)}, u32[]{:S(2)}) copy-start(f32[3,256]{1,0:T(4,128)} %slice.1837) | copy-start | bytes 9220
  564.3 53.4 %copy-start.118 = (f32[7,256]{1,0:T(8,128)S(1)}, f32[7,256]{1,0:T(8,128)}, u32[]{:S(2)}) copy-start(f32[7,256]{1,0:T(8,128)} %slice.1788) | copy-start | bytes 21508
  564.3 53.4 %copy-start.119 = (f32[7,256]{1,0:T(8,128)S(1)}, f32[7,256]{1,0:T(8,128)}, u32[]{:S(2)}) copy-start(f32[7,256]{1,0:T(8,128)} %slice.1835) | copy-start | bytes 21508
  564.3 53.4 %copy-start.120 = (f32[7,256]{1,0:T(8,128)S(1)}, f32[7,256]{1,0:T(8,128)}, u32[]{:S(2)}) copy-start(f32[7,256]{1,0:T(8,128)} %slice.1839) | copy-start | bytes 21508
  571.3 50.7 %copy-start.101 = (f32[31,256]{1,0:T(8,128)S(1)}, f32[31,256]{1,0:T(8,128)}, u32[]{:S(2)}) copy-start(f32[31,256]{1,0:T(8,128)} %slice.1768) | copy-start | bytes 95236
  571.3 50.7 %copy-start.102 = (f32[31,256]{1,0:T(8,128)S(1)}, f32[31,256]{1,0:T(8,128)}, u32[]{:S(2)}) copy-start(f32[31,256]{1,0:T(8,128)} %slice.1847) | copy-start | bytes 95236
  571.3 50.7 %copy-start.103 = (f32[31,256]{1,0:T(8,128)S(1)}, f32[31,256]{1,0:T(8,128)}, u32[]{:S(2)}) copy-start(f32[31,256]{1,0:T(8,128)} %slice.1851) | copy-start | bytes 95236
  571.3 50.7 %copy-start.104 = (f32[31,256]{1,0:T(8,128)S(1)}, f32[31,256]{1,0:T(8,128)}, u32[]{:S(2)}) copy-start(f32[31,256]{1,0:T(8,128)} %slice.1855) | copy-start | bytes 95236
  640.6 39.8 %copy-start.60 = (f32[128,512]{0,1:T(8,128)S(1)}, f32[128,512]{0,1:T(8,128)}, u32[]{:S(2)}) copy-start(f32[128,512]{0,1:T(8,128)} %add.1246) | copy-start | bytes 786436
  642.9 39.0 %copy-start.114 = (f32[512]{0:T(512)S(1)}, f32[512]{0:T(512)}, u32[]{:S(2)}) copy-start(f32[512]{0:T(512)} %copy-done.113) | copy-start | bytes 6148
  642.9 39.0 %copy-start.116 = (f32[512]{0:T(512)S(1)}, f32[512]{0:T(512)}, u32[]{:S(2)}) copy-start(f32[512]{0:T(512)} %copy-done.115) | copy-start | bytes 6148
  749.4 33.6 %copy-start.110 = (f32[512]{0:T(512)S(1)}, f32[512]{0:T(512)}, u32[]{:S(2)}) copy-start(f32[512]{0:T(512)} %copy-done.109) | copy-start | bytes 6148
  749.4 33.6 %copy-start.112 = (f32[512]{0:T(512)S(1)}, f32[512]{0:T(512)}, u32[]{:S(2)}) copy-start(f32[512]{0:T(512)} %copy-done.111) | copy-start | bytes 6148
  749.4 33.6 %copy-start.144 = (f32[4]{0:T(128)S(1)}, f32[4]{0:T(128)}, u32[]{:S(2)}) copy-start(f32[4]{0:T(128)} %get-tuple-element.315) | copy-start | bytes 52
  749.4 33.6 %copy-start.151 = (pred[4]{0:T(512)(128)(4,1)S(1)}, pred[4]{0:T(512)(128)(4,1)}, u32[]{:S(2)}) copy-start(pred[4]{0:T(512)(128)(4,1)} %iota_compare_fusion.1) | copy-start | bytes 16
  749.4 33.7 %copy-start.140 = (f32[128]{0:T(128)S(1)}, f32[128]{0:T(128)}, u32[]{:S(2)}) copy-start(f32[128]{0:T(128)} %copy-done.139) | copy-start | bytes 1540
  812.5 2.7 collective-permute-start
  813.8 5.7 collective-permute-start.1
  (128 other events, 1017.7 us)
Sparse Core Ops, SparseCore 0:
  8.9 61.8 all-gather.13
  72.4 57.7 all-gather.11
  131.8 57.7 all-gather.15
  823.3 18.7 reduce-scatter.1
where the time goes:
time: 863 us; the launch traced here: 851 us
  local copies, waits for them, and re-layouts  585 us (68%)
  blocking collectives  120 us (14%)
  other arithmetic  82.7 us (10%)
  waiting for transfers between devices  25.3 us (3%)
  between operations  18.7 us (2%)
  matrix products  15.3 us (2%)
    slice x322, local copies, waits for them, and re-layouts, block_pass(): lax.associative_scan(pair_combine, (decay_real, decay_quad, kick_real, im...  448 us
    all_gather x8, blocking collectives, on_device(): lax.all_gather(tuple((item[None] for item in forward_ends + backward_ends...  86.1 us
    pad x96, local copies, waits for them, and re-layouts, block_pass(): lax.associative_scan(pair_combine, (decay_real, decay_quad, kick_real, im...  77.6 us
    unnamed x337, local copies, waits for them, and re-layouts  21.9 us
    reduce_scatter x1, waiting for transfers between devices, on_device(): lax.psum_scatter(terms.astype(jnp.bfloat16), 'tp', scatter_dimension=1, t...  18.9 us
  transfers between devices with their start and end apart: 6, of which 2 were waited for; matrix products, arithmetic and copies ran while one was open for 80% of the time, Pallas kernels for 0%

commit v1 on v0

v1 whole, which is shorter than its diff:
```python
import functools

import jax
import jax.numpy as jnp
from jax import lax
from jax.experimental import pallas as pl
from jax.experimental.pallas import tpu as pltpu
from jax.sharding import PartitionSpec as P

GROUP = 16
LANES = 128
epsilon = 1e-06
f32 = jnp.float32
bf16 = jnp.bfloat16


def sin_cos(angle):
    turns = jnp.round(angle * 0.6366197723675814)
    r = angle - turns * 1.5703125
    r = r - turns * 4.837512969970703125e-4
    r = r - turns * 7.54978995489188216e-8
    z = r * r
    s = ((-1.9515295891e-4 * z + 8.3321608736e-3) * z - 1.6666654611e-1) * z * r + r
    c = ((2.443315711809948e-5 * z - 1.388731625493765e-3) * z + 4.166664568298827e-2) * z * z - 0.5 * z + 1.0
    quadrant = turns.astype(jnp.int32)
    odd = (quadrant & 1) == 1
    sin = jnp.where(odd, c, s)
    cos = jnp.where(odd, s, c)
    sin = jnp.where((quadrant & 2) == 2, -sin, sin)
    cos = jnp.where(((quadrant + 1) & 2) == 2, -cos, cos)
    return sin, cos


def decay_of(rate, turn, span):
    shrink = jnp.exp(-rate * span)
    sin, cos = sin_cos(turn * span)
    return shrink * cos, shrink * sin


def times(ar, ai, br, bi):
    return ar * br - ai * bi, ar * bi + ai * br


def split(value):
    high = value.astype(bf16)
    return high, (value - high.astype(f32)).astype(bf16)


def dot(a, b):
    return jnp.dot(a, b, preferred_element_type=f32)


def dot_nt(a, b):
    return lax.dot_general(a, b, (((1,), (1,)), ((), ())), preferred_element_type=f32)


def kernel(
    n, nt, starts,
    spacing, x_ref, rt_ref, drive_ref, read_ref, skip_ref, ov_ref, og_ref, stream_ref, gain_ref,
    taps_ref, upv_ref, upg_ref, down_ref,
    out_ref,
    upv, upg, down, kick, dec, ends, mix, mid, gain, pre, part, got, sums, done,
    w_send, w_recv, w_local, e_send, e_recv, g_send, g_recv, m_send, m_recv,
    z_send, z_recv, t_send, t_recv, p_send, p_recv, s_send, s_recv,
):
    me, mt = lax.axis_index("sp"), lax.axis_index("tp")
    tokens = x_ref.shape[0]
    groups = rt_ref.shape[2]
    channels = x_ref.shape[1] // 2
    width = upv.shape[1]
    rows = upv_ref.shape[0]
    cols = out_ref.shape[1]
    limit = upv_ref.shape[1] - width

    def remote(src, dst, send, recv, axis, peer):
        return pltpu.make_async_remote_copy(
            src_ref=src, dst_ref=dst, send_sem=send, recv_sem=recv,
            device_id={axis: peer}, device_id_type=pl.DeviceIdType.MESH)

    def start_of(index):
        return pl.multiple_of(jnp.minimum(index * width, limit), LANES)

    barrier = pltpu.get_barrier_semaphore()
    for offset in range(1, n):
        pl.semaphore_signal(barrier, inc=1, device_id={"sp": lax.rem(me + offset, n)},
                            device_id_type=pl.DeviceIdType.MESH)
    for offset in range(1, nt):
        pl.semaphore_signal(barrier, inc=1, device_id={"tp": lax.rem(mt + offset, nt)},
                            device_id_type=pl.DeviceIdType.MESH)
    pl.semaphore_wait(barrier, n + nt - 2)

    def weight_parts(which, target, slot):
        begin = start_of(target)
        place = pl.ds(pl.multiple_of(slot * rows, rows), rows)
        if which == 0:
            return upv_ref.at[:, pl.ds(begin, width)], upv.at[place, :]
        if which == 1:
            return upg_ref.at[:, pl.ds(begin, width)], upg.at[place, :]
        return (down_ref.at[pl.ds(begin, width), :],
                down.at[slot])

    def weight_copy(which, target, slot):
        src, dst = weight_parts(which, target, slot)
        return remote(src, dst, w_send.at[which, target], w_recv.at[which, slot], "sp", target)

    def weight_start(which):
        for offset in range(1, n):
            weight_copy(which, lax.rem(me + offset, n), me).start()

    def weight_wait(which):
        for offset in range(1, n):
            peer = lax.rem(me + offset, n)
            weight_copy(which, peer, me).wait_send()
            weight_copy(which, me, peer).wait_recv()
        src, dst = weight_parts(which, me, me)
        pltpu.make_async_copy(src, dst, w_local.at[which]).wait()

    for which in range(3):
        src, dst = weight_parts(which, me, me)
        pltpu.make_async_copy(src, dst, w_local.at[which]).start()

    def gain_copy(target, slot):
        return remote(gain_ref, gain.at[slot], g_send.at[target], g_recv.at[slot], "tp", target)

    for offset in range(1, nt):
        gain_copy(lax.rem(mt + offset, nt), mt).start()
    gain[mt] = gain_ref[...]

    x = x_ref[...]
    lane_group = lax.rem(lax.broadcasted_iota(jnp.int32, x.shape, 1), channels) // GROUP
    for d in range(2):
        high, low = split(drive_ref[d])
        for g in range(groups):
            picked = jnp.where(lane_group == g, x, jnp.zeros_like(x))
            pushed = dot(picked, high) + dot(picked, low)
            place = pl.ds(g, tokens, stride=groups)
            kick[d, 0, place, :] = pushed[:, :LANES]
            kick[d, 1, place, :] = pushed[:, LANES:]

    rates = [rt_ref[0, d] for d in range(2)]
    turns = [rt_ref[1, d] for d in range(2)]
    inverse = []
    for d in range(2):
        square = rates[d] * rates[d] + turns[d] * turns[d]
        inverse.append((-rates[d] / square, -turns[d] / square))

    def spot(d, i):
        return i if d == 0 else tokens - 1 - i

    def first(i, carry):
        state, total = list(carry[:4]), carry[4]
        for d in range(2):
            t = spot(d, i)
            step = spacing[t]
            if d == 0:
                total = total + step
            place = pl.ds(pl.multiple_of(t * groups, groups), groups)
            dr, di = decay_of(rates[d], turns[d], step)
            cr, ci = times(dr - 1.0, di, *inverse[d])
            kr, ki = times(cr, ci, kick[d, 0, place, :], kick[d, 1, place, :])
            dec[d, 0, place, :] = dr
            dec[d, 1, place, :] = di
            kick[d, 0, place, :] = kr
            kick[d, 1, place, :] = ki
            ar, ai = times(dr, di, state[2 * d], state[2 * d + 1])
            state[2 * d], state[2 * d + 1] = ar + kr, ai + ki
        return (*state, total)

    zero = jnp.zeros((groups, LANES), f32)
    found = lax.fori_loop(0, tokens, first, (zero, zero, zero, zero, jnp.float32(0.0)), unroll=4)
    for d in range(2):
        ar, ai = decay_of(rates[d], turns[d], found[4])
        ends[me, d, 0] = found[2 * d]
        ends[me, d, 1] = found[2 * d + 1]
        ends[me, d, 2] = ar
        ends[me, d, 3] = ai

    def ends_copy(target, slot):
        return remote(ends.at[slot], ends.at[slot], e_send.at[target], e_recv.at[slot], "sp", target)

    for offset in range(1, n):
        ends_copy(lax.rem(me + offset, n), me).start()
    weight_start(0)
    weight_start(1)
    for offset in range(1, n):
        peer = lax.rem(me + offset, n)
        ends_copy(peer, me).wait_send()
        ends_copy(me, peer).wait_recv()

    carry = []
    for d in range(2):
        cr, ci = zero, zero
        for k in range(n):
            s = k if d == 0 else n - 1 - k
            use = (s < me) if d == 0 else (s > me)
            nr, ni = times(ends[s, d, 2], ends[s, d, 3], cr, ci)
            flag = jnp.where(use, 1, 0)
            keep = jnp.full((groups, LANES), flag, jnp.int32) == 1
            cr = jnp.where(keep, nr + ends[s, d, 0], cr)
            ci = jnp.where(keep, ni + ends[s, d, 1], ci)
        carry += [cr, ci]

    def second(i, carry):
        state = list(carry)
        for d in range(2):
            t = spot(d, i)
            place = pl.ds(pl.multiple_of(t * groups, groups), groups)
            ar, ai = times(dec[d, 0, place, :], dec[d, 1, place, :], state[2 * d], state[2 * d + 1])
            state[2 * d] = ar + kick[d, 0, place, :]
            state[2 * d + 1] = ai + kick[d, 1, place, :]
            kick[d, 0, place, :] = state[2 * d]
            kick[d, 1, place, :] = state[2 * d + 1]
        return tuple(state)

    lax.fori_loop(0, tokens, second, tuple(carry), unroll=4)

    reading = skip_ref[...] * x.astype(f32)
    for d in range(2):
        high, low = split(read_ref[d])
        for g in range(groups):
            place = pl.ds(g, tokens, stride=groups)
            state = jnp.concatenate([kick[d, 0, place, :], kick[d, 1, place, :]], axis=1)
            state_high, state_low = split(state)
            value = dot_nt(state_high, high) + dot_nt(state_low, high) + dot_nt(state_high, low)
            reading = reading + jnp.where(lane_group == g, value, 0.0)
    mix[mt] = jax.nn.gelu(reading).astype(bf16)

    def mix_copy(target, slot):
        return remote(mix.at[slot], mix.at[slot], m_send.at[target], m_recv.at[slot], "tp", target)

    for offset in range(1, nt):
        mix_copy(lax.rem(mt + offset, nt), mt).start()
    for offset in range(1, nt):
        peer = lax.rem(mt + offset, nt)
        mix_copy(peer, mt).wait_send()
        mix_copy(mt, peer).wait_recv()

    value = jnp.zeros((tokens, cols), f32)
    gate = jnp.zeros((tokens, cols), f32)
    half = ov_ref.shape[0] // 2
    for k in range(nt):
        for h in range(2):
            piece = mix[k][:, h * channels:(h + 1) * channels]
            at = slice(h * half + k * channels, h * half + (k + 1) * channels)
            value = value + dot(piece, ov_ref[at, :])
            gate = gate + dot(piece, og_ref[at, :])
    mid[me, mt] = (stream_ref[...].astype(f32) + value * jax.nn.sigmoid(gate)).astype(bf16)

    def z_copy(target, slot):
        return remote(mid.at[slot, mt], mid.at[slot, mt], z_send.at[target], z_recv.at[slot], "sp", target)

    def t_copy(s, target, slot):
        return remote(mid.at[s, slot], mid.at[s, slot], t_send.at[s, target], t_recv.at[s, slot], "tp", target)

    for offset in range(1, n):
        z_copy(lax.rem(me + offset, n), me).start()
    for offset in range(1, nt):
        t_copy(me, lax.rem(mt + offset, nt), mt).start()
    weight_start(2)
    for offset in range(1, n):
        peer = lax.rem(me + n - offset, n) if offset % 2 else lax.rem(me + offset, n)
        peer = lax.rem(me + offset, n)
        z_copy(me, peer).wait_recv()
        for other in range(1, nt):
            t_copy(peer, lax.rem(mt + other, nt), mt).start()
    for offset in range(1, nt):
        peer = lax.rem(mt + offset, nt)
        gain_copy(peer, mt).wait_send()
        gain_copy(mt, peer).wait_recv()
    weight_wait(0)
    weight_wait(1)
    for offset in range(1, n):
        z_copy(lax.rem(me + offset, n), me).wait_send()

    for i in range(2):
        pre[pl.ds(i * (8 + n * tokens), 8), :] = jnp.zeros((8, 2 * width), f32)
    for step in range(n):
        s = lax.rem(me + step, n)
        for offset in range(1, nt):
            peer = lax.rem(mt + offset, nt)
            t_copy(s, peer, mt).wait_send()
            t_copy(s, mt, peer).wait_recv()
        squares = jnp.zeros((tokens, 1), f32)
        for k in range(nt):
            piece = mid[s, k].astype(f32)
            squares = squares + jnp.sum(piece * piece, axis=1, keepdims=True)
        scale = lax.rsqrt(squares / (nt * cols) + epsilon)
        normed = jnp.concatenate(
            [(mid[s, k].astype(f32) * scale * gain[k]).astype(bf16) for k in range(nt)], axis=1)
        place = pl.ds(pl.multiple_of(8 + s * tokens, 8), tokens)
        pre[place, :width] = dot(normed, upv[...]).astype(bf16).astype(f32)
        pre[place, width:] = dot(normed, upg[...]).astype(bf16).astype(f32)

    weight_wait(2)
    begin = start_of(me)
    own_from = me * width - begin
    valid = lax.broadcasted_iota(jnp.int32, (1, width), 1) >= own_from

    def conv_of(k, s):
        base = pl.multiple_of(s * tokens, 8)
        block = pre[pl.ds(base, tokens + 16), k * width:(k + 1) * width]
        tap = taps_ref[k, :, pl.ds(begin, width)]
        return (tap[0:1] * block[7:7 + tokens] + tap[1:2] * block[8:8 + tokens]
                + tap[2:3] * block[9:9 + tokens])

    def p_copy(s, target, slot):
        return remote(part.at[s, target], got.at[s, slot], p_send.at[s, target], p_recv.at[s, slot],
                      "tp", target)

    for step in range(n):
        s = lax.rem(me + 1 + step, n)
        conv_value, conv_gate = conv_of(0, s), conv_of(1, s)
        hidden = conv_gate * jax.nn.sigmoid(conv_gate) * conv_value
        hidden = jnp.where(valid, hidden, 0.0).astype(bf16)
        per = down.shape[2]
        for k in range(n):
            terms = dot(hidden, down[k]).astype(bf16)
            if per >= cols:
                for j in range(per // cols):
                    part[s, k * (per // cols) + j] = terms[:, j * cols:(j + 1) * cols]
            else:
                ratio = cols // per
                part[s, k // ratio, :, (k % ratio) * per:(k % ratio + 1) * per] = terms
        for offset in range(1, nt):
            p_copy(s, lax.rem(mt + offset, nt), mt).start()

    def s_copy(target, slot):
        return remote(sums.at[target], done.at[slot], s_send.at[target], s_recv.at[slot], "sp", target)

    own = None
    for step in range(n):
        s = lax.rem(me + 1 + step, n)
        total = part[s, mt].astype(f32)
        for offset in range(1, nt):
            peer = lax.rem(mt + offset, nt)
            p_copy(s, peer, mt).wait_send()
            p_copy(s, mt, peer).wait_recv()
            total = total + got[s, peer].astype(f32)
        if step < n - 1:
            sums[s] = total.astype(bf16)
            s_copy(s, me).start()
        else:
            own = total
    for offset in range(1, n):
        peer = lax.rem(me + offset, n)
        s_copy(peer, me).wait_send()
        s_copy(me, peer).wait_recv()
        own = own + done[peer].astype(f32)
    out_ref[...] = (mid[me, mt].astype(f32) + own).astype(bf16)


def packed(wide, narrow):
    def halves(value):
        states = value.shape[3] // 2
        flat = value.reshape(2, -1, 2 * states)
        return flat[..., :states], flat[..., states:]

    wide_parts, narrow_parts = halves(wide), halves(narrow)
    count, states = wide_parts[0].shape[1:]
    small = narrow_parts[0].shape[2]
    top = jnp.concatenate(
        [jnp.pad(part, ((0, 0), (0, 0), (0, LANES - states))) for part in wide_parts], axis=2)
    low = jnp.concatenate(
        [jnp.pad(part, ((0, 0), (0, 0), (states, LANES - states - small))) for part in narrow_parts],
        axis=2)
    return jnp.concatenate([top, low], axis=1)


def on_device(
    n, nt,
    input_wide, input_narrow, spacing, rate_wide, turn_wide, drive_wide, read_wide,
    narrow_decay_rate, turn_narrow, drive_narrow, read_narrow, skip_gain, out_value, out_gate,
    stream, norm_gain, up_value, up_gate, conv_taps, down_weight,
):
    tokens = spacing.shape[0]
    groups = rate_wide.shape[1]
    x = jnp.concatenate([input_wide, input_narrow], axis=1)
    rest = LANES - rate_wide.shape[2] - narrow_decay_rate.shape[2]
    ones = jnp.ones((2, groups, rest), f32)
    rt = jnp.stack([jnp.concatenate([rate_wide, narrow_decay_rate, ones], axis=2),
                    jnp.concatenate([turn_wide, turn_narrow, ones], axis=2)])
    drive = packed(drive_wide, drive_narrow)
    read = packed(read_wide, read_narrow)
    skip = skip_gain.reshape(1, -1)
    extra = -up_value.shape[1] % LANES
    if extra:
        up_value = jnp.pad(up_value, ((0, 0), (0, extra)))
        up_gate = jnp.pad(up_gate, ((0, 0), (0, extra)))
        conv_taps = jnp.pad(conv_taps, ((0, 0), (0, 0), (0, extra)))
        down_weight = jnp.pad(down_weight, ((0, extra), (0, 0)))
    hidden = up_value.shape[1]
    width = -(-hidden // (n * LANES)) * LANES
    rows = up_value.shape[0]
    cols = stream.shape[1]
    per = down_weight.shape[1]
    vmem = pl.BlockSpec(memory_space=pltpu.VMEM)
    anywhere = pl.BlockSpec(memory_space=pl.ANY)
    dma = pltpu.SemaphoreType.DMA
    return pl.pallas_call(
        functools.partial(kernel, n, nt, None),
        out_shape=jax.ShapeDtypeStruct((tokens, cols), bf16),
        in_specs=[pl.BlockSpec(memory_space=pltpu.SMEM)] + [vmem] * 10 + [anywhere] * 3,
        out_specs=vmem,
        scratch_shapes=[
            pltpu.VMEM((rows * n, width), bf16),
            pltpu.VMEM((rows * n, width), bf16),
            pltpu.VMEM((n, width, per), bf16),
            pltpu.VMEM((2, 2, tokens * groups, LANES), f32),
            pltpu.VMEM((2, 2, tokens * groups, LANES), f32),
            pltpu.VMEM((n, 2, 4, groups, LANES), f32),
            pltpu.VMEM((nt, tokens, x.shape[1]), bf16),
            pltpu.VMEM((n, nt, tokens, cols), bf16),
            pltpu.VMEM((nt, 1, cols), f32),
            pltpu.VMEM((n * tokens + 16, 2 * width), f32),
            pltpu.VMEM((n, nt, tokens, cols), bf16),
            pltpu.VMEM((n, nt, tokens, cols), bf16),
            pltpu.VMEM((n, tokens, cols), bf16),
            pltpu.VMEM((n, tokens, cols), bf16),
            dma((3, n)), dma((3, n)), dma((3,)),
            dma((n,)), dma((n,)),
            dma((nt,)), dma((nt,)),
            dma((nt,)), dma((nt,)),
            dma((n,)), dma((n,)),
            dma((n, nt)), dma((n, nt)),
            dma((n, nt)), dma((n, nt)),
            dma((n,)), dma((n,)),
        ],
        compiler_params=pltpu.CompilerParams(
            collective_id=0, has_side_effects=True, vmem_limit_bytes=60 * 1024 * 1024),
    )(spacing, x, rt, drive, read, skip, out_value, out_gate, stream, norm_gain.reshape(1, -1),
      conv_taps, up_value, up_gate, down_weight)


def solution(mesh):
    placed = (
        P(("grp", "sp"), "tp"),
        P(("grp", "sp"), "tp"),
        P(("grp", "sp")),
        P(None, "tp", None),
        P(None, "tp", None),
        P(None, "tp", None, None),
        P(None, "tp", None, None),
        P(None, "tp", None),
        P(None, "tp", None),
        P(None, "tp", None, None),
        P(None, "tp", None, None),
        P(None, "tp"),
        P(None, "tp"),
        P(None, "tp"),
        P(("grp", "sp"), "tp"),
        P("tp"),
        P("sp", "tp"),
        P("sp", "tp"),
        P(None, None, "tp"),
        P("tp", "sp"),
    )
    return jax.shard_map(
        functools.partial(on_device, mesh.shape["sp"], mesh.shape["tp"]),
        mesh=mesh, in_specs=placed, out_specs=P(("grp", "sp"), "tp"), check_vma=False
    )
```

time: 863 us -> 96.6 us (0.11); the launches traced: 851 us -> 96 us
  local copies, waits for them, and re-layouts: 585 us -> 5.83 us
  blocking collectives: 120 us -> 0 us
  Pallas kernels: 0 us -> 86.5 us
  other arithmetic: 82.7 us -> 3.53 us
  waiting for transfers between devices: 25.3 us -> 0 us
  between operations: 18.7 us -> 0.12 us
  matrix products: 15.3 us -> 0 us
    slice x328 -> x4, local copies, waits for them, and re-layouts: 448 us -> 0.36 us  [halves(): return (flat[..., :states], flat[..., states:])]
    all_gather x11 -> x0, blocking collectives: 103 us -> none  [the longest x8 86.1 us: on_device(): lax.all_gather(tuple((item[None] for item in forward_ends + backward_ends...]
    pallas_call x0 -> x1, Pallas kernels: none -> 86.5 us  [on_device(): pl.pallas_call(functools.partial(kernel, n, nt, None), out_shape=jax.Shap...]
    pad x96 -> x0, local copies, waits for them, and re-layouts: 77.6 us -> none  [block_pass(): lax.associative_scan(pair_combine, (decay_real, decay_quad, kick_real, im...]
    add x104 -> x0, other arithmetic: 38.4 us -> none  [the longest x36 13.9 us: pair_combine(): moved_quad + later[3]]
    mul x33 -> x0, local copies, waits for them, and re-layouts: 22 us -> none  [the longest x6 6.6 us: complex_times(): left_real * right_quad + left_quad * right_real]
    reduce_scatter x1 -> x0, waiting for transfers between devices: 18.9 us -> none  [on_device(): lax.psum_scatter(terms.astype(jnp.bfloat16), 'tp', scatter_dimension=1, t...]
    unnamed x337 -> x26, local copies, waits for them, and re-layouts: 21.9 us -> 5.4 us
  transfers between devices with their start and end apart: 6 -> 0, of which waited for: 2 -> 0; matrix products, arithmetic and copies ran while one was open for 80% -> 0% of each run, Pallas kernels for 0% -> 0%
where the time goes in v1:
time: 96.6 us; the launch traced here: 96 us
  Pallas kernels  86.5 us (90%)
  local copies, waits for them, and re-layouts  5.83 us (6%)
  other arithmetic  3.53 us (4%)
    pallas_call x1, Pallas kernels, on_device(): pl.pallas_call(functools.partial(kernel, n, nt, None), out_shape=jax.Shap...  86.5 us
    unnamed x26, local copies, waits for them, and re-layouts  5.4 us

profile of v1, /device:TPU:0, one launch (start us, length us, event | category | flops | bytes accessed | tf_op | source)
XLA Modules:
  0.0 96.0 jit_solution(10918830743357558911)
XLA Ops:
  0.0 0.7 copy-done.11
  0.7 1.0 %broadcast_select_fusion = (f32[2,128,128]{2,1,0:T(8,128)S(1)}, f32[2,128,128]{2,1,0:T(8,128)S(1)}) fusion(pred[128]{0:T(512)(128)(4,1)S(1)} %copy-done.11, f32[2,8,16,128]{3,2,1,0:T(8,128)} %param.26, f32[2,8,16,128]{3,2,1,0:T(8,128)} %param.25), kind=kLoop, calls=%fused_computation.14 | loop fusion | flops 65536 | bytes 524416 | tf_op jit(solution)/shard_map/jit(_pad)/pad | solution.py:362
  1.7 0.0 copy-done.2
  1.7 0.0 copy-start.3
  1.7 0.1 fusion.5
  1.8 0.8 copy-done.3
  2.6 0.1 fusion.6
  2.7 0.8 copy-done
  3.5 0.1 slice.28
  3.6 0.8 copy-done.1
  4.4 0.1 slice.31
  4.5 0.0 copy-start.7
  4.5 0.0 copy-start.8
  4.5 0.0 copy-start.9
  4.5 0.0 copy-start.10
  4.6 1.2 %fusion = (f32[2,256,256]{2,1,0:T(8,128)}, f32[2,256,256]{2,1,0:T(8,128)}) fusion(f32[2,128,32]{2,1,0:T(8,128)S(1)} %get-tuple-element.6, f32[2,128,32]{2,1,0:T(8,128)S(1)} %get-tuple-element.5, f32[2,128,64]{2,1,0:T(8,128)S(1)} %slice.31, f32[2,128,128]{2,1,0:T(8,128)S(1)} %get-tuple-element.9, f32[2,128,32]{2,1,0:T(8,128)S(1)} %get-tuple-element.8, ...), kind=kLoop, calls=%fused_computation.1 | loop fusion | flops 3276800 | bytes 1572864 | tf_op jit(solution)/shard_map/concatenate | solution.py:366
  5.7 0.1 pad.49.clone
  5.8 0.0 copy-done.7
  5.8 0.0 copy-done.8
  5.8 0.0 copy-done.9
  5.8 0.0 copy-done.10
  5.8 0.0 copy-start.5
  5.8 0.0 copy-start.6
  5.9 0.1 maximum_bitcast_fusion
  5.9 0.6 pad_maximum_fusion.1.rt_ref
  6.5 0.1 copy-done.5
  6.6 0.0 copy-done.6
  6.6 0.6 pad_maximum_fusion.x_ref
  7.3 0.1 copy-done.4
  7.4 0.6 copy.21.taps_ref
  8.0 86.5 %shard_map.190 = bf16[128,256]{1,0:T(8,128)(2,1)} custom-call(f32[128]{0:T(128)} %spacing.1, bf16[128,256]{1,0:T(8,128)(2,1)} %pad_maximum_fusion.x_ref, f32[2,2,8,128]{3,2,1,0:T(8,128)} %pad_maximum_fusion.1.rt_ref, f32[2,256,256]{2,1,0:T(8,128)} %get-tuple-element.14.drive_ref, f32[2,256,256]{2,1,0:T(8,128)} %get-tuple-element.13.read_ref, ...), custom_call_target="tpu_custom_call" | custom-call | tf_op jit(solution)/shard_map/pallas_call | solution.py:399
  94.5 1.5 %copy.23 = bf16[128,256]{1,0:T(8,128)(2,1)} copy(bf16[128,256]{1,0:T(8,128)(2,1)} %shard_map.190) | data formatting | bytes 131072
  (6 shorter events, 0.0 us)
Async XLA Ops:
  0.0 0.7 copy-start.11
  0.7 1.0 %copy-start.2 = (f32[2,8,16,64]{3,2,1,0:T(8,128)S(1)}, f32[2,8,16,64]{3,2,1,0:T(8,128)}, u32[]{:S(2)}) copy-start(f32[2,8,16,64]{3,2,1,0:T(8,128)} %param.30) | copy-start | bytes 196612
  1.7 0.9 copy-start.3
  2.6 0.9 copy-start
  3.5 0.9 copy-start.1
  4.5 1.3 %copy-start.7 = (f32[2,8,32]{2,1,0:T(8,128)S(1)}, f32[2,8,32]{2,1,0:T(8,128)}, u32[]{:S(2)}) copy-start(f32[2,8,32]{2,1,0:T(8,128)} %param.27) | copy-start | bytes 6148
  4.5 1.3 %copy-start.8 = (f32[2,8,64]{2,1,0:T(8,128)S(1)}, f32[2,8,64]{2,1,0:T(8,128)}, u32[]{:S(2)}) copy-start(f32[2,8,64]{2,1,0:T(8,128)} %param.23) | copy-start | bytes 12292
  4.5 1.3 %copy-start.9 = (f32[2,8,32]{2,1,0:T(8,128)S(1)}, f32[2,8,32]{2,1,0:T(8,128)}, u32[]{:S(2)}) copy-start(f32[2,8,32]{2,1,0:T(8,128)} %param.28) | copy-start | bytes 6148
  4.5 1.3 %copy-start.10 = (f32[2,8,64]{2,1,0:T(8,128)S(1)}, f32[2,8,64]{2,1,0:T(8,128)}, u32[]{:S(2)}) copy-start(f32[2,8,64]{2,1,0:T(8,128)} %param.24) | copy-start | bytes 12292
  5.8 0.8 copy-start.5
  5.8 0.8 copy-start.6
  6.6 0.8 copy-start.4

commit v2 on v1

--- a/solution.py
+++ b/solution.py
@@ -55,15 +55,17 @@
 
 
 def kernel(
-    n, nt, starts,
+    n, nt, ng,
     spacing, x_ref, rt_ref, drive_ref, read_ref, skip_ref, ov_ref, og_ref, stream_ref, gain_ref,
     taps_ref, upv_ref, upg_ref, down_ref,
     out_ref,
-    upv, upg, down, kick, dec, ends, mix, mid, gain, pre, part, got, sums, done,
-    w_send, w_recv, w_local, e_send, e_recv, g_send, g_recv, m_send, m_recv,
-    z_send, z_recv, t_send, t_recv, p_send, p_recv, s_send, s_recv,
+    upv, upg, down, kick, dec, ends, mix, mid, gain, pre, part, near, got, own, sums, done,
+    w_send, w_recv, w_local, y_send, y_recv, e_send, e_recv, g_send, g_recv, m_send, m_recv,
+    z_send, z_recv, t_send, f_send, t_recv, d_send, d_recv, p_send, p_recv, s_send, s_recv,
 ):
-    me, mt = lax.axis_index("sp"), lax.axis_index("tp")
+    me, mt, mg = lax.axis_index("sp"), lax.axis_index("tp"), lax.axis_index("grp")
+    partner = mt + 1 - 2 * lax.rem(mt, 2)
+    side = nt // 2
     tokens = x_ref.shape[0]
     groups = rt_ref.shape[2]
     channels = x_ref.shape[1] // 2
@@ -87,21 +89,39 @@
     for offset in range(1, nt):
         pl.semaphore_signal(barrier, inc=1, device_id={"tp": lax.rem(mt + offset, nt)},
                             device_id_type=pl.DeviceIdType.MESH)
-    pl.semaphore_wait(barrier, n + nt - 2)
-
-    def weight_parts(which, target, slot):
+    for offset in range(1, ng):
+        pl.semaphore_signal(barrier, inc=1, device_id={"grp": lax.rem(mg + offset, ng)},
+                            device_id_type=pl.DeviceIdType.MESH)
+    pl.semaphore_wait(barrier, n + nt + ng - 3)
+
+    def weight_parts(which, target, slot, index, count):
         begin = start_of(target)
-        place = pl.ds(pl.multiple_of(slot * rows, rows), rows)
-        if which == 0:
-            return upv_ref.at[:, pl.ds(begin, width)], upv.at[place, :]
-        if which == 1:
-            return upg_ref.at[:, pl.ds(begin, width)], upg.at[place, :]
-        return (down_ref.at[pl.ds(begin, width), :],
-                down.at[slot])
+        full = width if which == 2 else rows
+        size = full // count
+        first_row = pl.multiple_of(index * size, size)
+        if which == 2:
+            return (down_ref.at[pl.ds(pl.multiple_of(begin + first_row, GROUP), size), :],
+                    down.at[slot, pl.ds(first_row, size), :])
+        source, held = ((upv_ref, upv), (upg_ref, upg))[which]
+        return (source.at[pl.ds(first_row, size), pl.ds(begin, width)],
+                held.at[pl.ds(pl.multiple_of(slot * rows + first_row, size), size), :])
 
     def weight_copy(which, target, slot):
-        src, dst = weight_parts(which, target, slot)
+        src, dst = weight_parts(which, target, slot, mg, ng)
         return remote(src, dst, w_send.at[which, target], w_recv.at[which, slot], "sp", target)
+
+    def share_copy(which, slot, index):
+        _, block = weight_parts(which, me, slot, index, ng)
+        offset = 1 if index is mg else 0
+        return remote(block, block, y_send.at[which, slot], y_recv.at[which, slot], "grp",
+                      lax.rem(mg + offset, ng))
+
+    def weight_share(which):
+        for offset in range(1, n):
+            peer = lax.rem(me + offset, n)
+            weight_copy(which, me, peer).wait_recv()
+            if ng == 2:
+                share_copy(which, peer, mg).start()
 
     def weight_start(which):
         for offset in range(1, n):
@@ -111,12 +131,15 @@
         for offset in range(1, n):
             peer = lax.rem(me + offset, n)
             weight_copy(which, peer, me).wait_send()
-            weight_copy(which, me, peer).wait_recv()
-        src, dst = weight_parts(which, me, me)
+            if ng == 2:
+                share_copy(which, peer, mg).wait_send()
+                share_copy(which, peer, 1 - mg).wait_recv()
+        src, dst = weight_parts(which, me, me, 0, 1)
         pltpu.make_async_copy(src, dst, w_local.at[which]).wait()
 
+    weight_start(0)
     for which in range(3):
-        src, dst = weight_parts(which, me, me)
+        src, dst = weight_parts(which, me, me, 0, 1)
         pltpu.make_async_copy(src, dst, w_local.at[which]).start()
 
     def gain_copy(target, slot):
@@ -180,7 +203,6 @@
 
     for offset in range(1, n):
         ends_copy(lax.rem(me + offset, n), me).start()
-    weight_start(0)
     weight_start(1)
     for offset in range(1, n):
         peer = lax.rem(me + offset, n)
@@ -199,6 +221,7 @@
             cr = jnp.where(keep, nr + ends[s, d, 0], cr)
             ci = jnp.where(keep, ni + ends[s, d, 1], ci)
         carry += [cr, ci]
+    weight_share(0)
 
     def second(i, carry):
         state = list(carry)
@@ -235,6 +258,7 @@
         mix_copy(peer, mt).wait_send()
         mix_copy(mt, peer).wait_recv()
 
+    weight_share(1)
     value = jnp.zeros((tokens, cols), f32)
     gate = jnp.zeros((tokens, cols), f32)
     half = ov_ref.shape[0] // 2
@@ -252,17 +276,30 @@
     def t_copy(s, target, slot):
         return remote(mid.at[s, slot], mid.at[s, slot], t_send.at[s, target], t_recv.at[s, slot], "tp", target)
 
+    def f_copy(s, slot):
+        return remote(mid.at[s, slot], mid.at[s, slot], f_send.at[s, slot], t_recv.at[s, slot], "tp", partner)
+
+    def spread(s):
+        for offset in range(1, side):
+            t_copy(s, lax.rem(mt + 2 * offset, nt), mt).start()
+        f_copy(s, mt).start()
+
+    def relay(s):
+        for offset in range(1, side):
+            peer = lax.rem(mt + 2 * offset, nt)
+            t_copy(s, mt, peer).wait_recv()
+            f_copy(s, peer).start()
+
     for offset in range(1, n):
         z_copy(lax.rem(me + offset, n), me).start()
-    for offset in range(1, nt):
-        t_copy(me, lax.rem(mt + offset, nt), mt).start()
+    spread(me)
     weight_start(2)
     for offset in range(1, n):
-        peer = lax.rem(me + n - offset, n) if offset % 2 else lax.rem(me + offset, n)
         peer = lax.rem(me + offset, n)
         z_copy(me, peer).wait_recv()
-        for other in range(1, nt):
-            t_copy(peer, lax.rem(mt + other, nt), mt).start()
+        spread(peer)
+        relay(lax.rem(me + offset - 1, n))
+    relay(lax.rem(me + n - 1, n))
     for offset in range(1, nt):
         peer = lax.rem(mt + offset, nt)
         gain_copy(peer, mt).wait_send()
@@ -271,15 +308,18 @@
     weight_wait(1)
     for offset in range(1, n):
         z_copy(lax.rem(me + offset, n), me).wait_send()
+    weight_share(2)
 
     for i in range(2):
         pre[pl.ds(i * (8 + n * tokens), 8), :] = jnp.zeros((8, 2 * width), f32)
     for step in range(n):
         s = lax.rem(me + step, n)
-        for offset in range(1, nt):
-            peer = lax.rem(mt + offset, nt)
-            t_copy(s, peer, mt).wait_send()
-            t_copy(s, mt, peer).wait_recv()
+        for offset in range(side):
+            peer = lax.rem(mt + 2 * offset, nt)
+            if offset:
+                t_copy(s, peer, mt).wait_send()
+            f_copy(s, peer).wait_send()
+            f_copy(s, lax.rem(partner + 2 * offset, nt)).wait_recv()
         squares = jnp.zeros((tokens, 1), f32)
         for k in range(nt):
             piece = mid[s, k].astype(f32)
@@ -303,9 +343,24 @@
         return (tap[0:1] * block[7:7 + tokens] + tap[1:2] * block[8:8 + tokens]
                 + tap[2:3] * block[9:9 + tokens])
 
+    def d_copy(s, target):
+        return remote(part.at[s, target], near.at[s, target], d_send.at[s, target], d_recv.at[s, target],
+                      "tp", partner)
+
     def p_copy(s, target, slot):
         return remote(part.at[s, target], got.at[s, slot], p_send.at[s, target], p_recv.at[s, slot],
                       "tp", target)
+
+    def pass_on(s):
+        for offset in range(side):
+            target = lax.rem(mt + 2 * offset, nt)
+            d_copy(s, target).wait_recv()
+            total = part[s, target].astype(f32) + near[s, target].astype(f32)
+            if offset:
+                part[s, target] = total.astype(bf16)
+                p_copy(s, target, mt).start()
+            else:
+                own[s] = total
 
     for step in range(n):
         s = lax.rem(me + 1 + step, n)
@@ -321,32 +376,34 @@
             else:
                 ratio = cols // per
                 part[s, k // ratio, :, (k % ratio) * per:(k % ratio + 1) * per] = terms
-        for offset in range(1, nt):
-            p_copy(s, lax.rem(mt + offset, nt), mt).start()
+        for offset in range(side):
+            d_copy(s, lax.rem(partner + 2 * offset, nt)).start()
+        if step:
+            pass_on(lax.rem(me + step, n))
+    pass_on(me)
 
     def s_copy(target, slot):
         return remote(sums.at[target], done.at[slot], s_send.at[target], s_recv.at[slot], "sp", target)
 
-    own = None
     for step in range(n):
         s = lax.rem(me + 1 + step, n)
-        total = part[s, mt].astype(f32)
-        for offset in range(1, nt):
-            peer = lax.rem(mt + offset, nt)
-            p_copy(s, peer, mt).wait_send()
-            p_copy(s, mt, peer).wait_recv()
-            total = total + got[s, peer].astype(f32)
+        total = own[s]
+        for offset in range(side):
+            d_copy(s, lax.rem(partner + 2 * offset, nt)).wait_send()
+            if offset:
+                peer = lax.rem(mt + 2 * offset, nt)
+                p_copy(s, peer, mt).wait_send()
+                p_copy(s, mt, peer).wait_recv()
+                total = total + got[s, peer].astype(f32)
         if step < n - 1:
             sums[s] = total.astype(bf16)
             s_copy(s, me).start()
-        else:
-            own = total
     for offset in range(1, n):
         peer = lax.rem(me + offset, n)
         s_copy(peer, me).wait_send()
         s_copy(me, peer).wait_recv()
-        own = own + done[peer].astype(f32)
-    out_ref[...] = (mid[me, mt].astype(f32) + own).astype(bf16)
+        total = total + done[peer].astype(f32)
+    out_ref[...] = (mid[me, mt].astype(f32) + total).astype(bf16)
 
 
 def packed(wide, narrow):
@@ -367,7 +424,7 @@
 
 
 def on_device(
-    n, nt,
+    n, nt, ng,
     input_wide, input_narrow, spacing, rate_wide, turn_wide, drive_wide, read_wide,
     narrow_decay_rate, turn_narrow, drive_narrow, read_narrow, skip_gain, out_value, out_gate,
     stream, norm_gain, up_value, up_gate, conv_taps, down_weight,
@@ -397,7 +454,7 @@
     anywhere = pl.BlockSpec(memory_space=pl.ANY)
     dma = pltpu.SemaphoreType.DMA
     return pl.pallas_call(
-        functools.partial(kernel, n, nt, None),
+        functools.partial(kernel, n, nt, ng),
         out_shape=jax.ShapeDtypeStruct((tokens, cols), bf16),
         in_specs=[pl.BlockSpec(memory_space=pltpu.SMEM)] + [vmem] * 10 + [anywhere] * 3,
         out_specs=vmem,
@@ -414,13 +471,16 @@
             pltpu.VMEM((n * tokens + 16, 2 * width), f32),
             pltpu.VMEM((n, nt, tokens, cols), bf16),
             pltpu.VMEM((n, nt, tokens, cols), bf16),
+            pltpu.VMEM((n, nt, tokens, cols), bf16),
+            pltpu.VMEM((n, tokens, cols), f32),
             pltpu.VMEM((n, tokens, cols), bf16),
             pltpu.VMEM((n, tokens, cols), bf16),
-            dma((3, n)), dma((3, n)), dma((3,)),
+            dma((3, n)), dma((3, n)), dma((3,)), dma((3, n)), dma((3, n)),
             dma((n,)), dma((n,)),
             dma((nt,)), dma((nt,)),
             dma((nt,)), dma((nt,)),
             dma((n,)), dma((n,)),
+            dma((n, nt)), dma((n, nt)), dma((n, nt)),
             dma((n, nt)), dma((n, nt)),
             dma((n, nt)), dma((n, nt)),
             dma((n,)), dma((n,)),
@@ -455,6 +515,6 @@
         P("tp", "sp"),
     )
     return jax.shard_map(
-        functools.partial(on_device, mesh.shape["sp"], mesh.shape["tp"]),
+        functools.partial(on_device, mesh.shape["sp"], mesh.shape["tp"], mesh.shape["grp"]),
         mesh=mesh, in_specs=placed, out_specs=P(("grp", "sp"), "tp"), check_vma=False
     )

time: 96.6 us -> 80.5 us (0.83)
  Pallas kernels: 86.5 us -> 70.6 us
    pallas_call x1, Pallas kernels: 86.5 us -> 70.6 us  [on_device(): pl.pallas_call(functools.partial(kernel, n, nt, ng), out_shape=jax.ShapeD...]
where the time goes in v2:
time: 80.5 us; the launch traced here: 80.1 us
  Pallas kernels  70.6 us (88%)
  local copies, waits for them, and re-layouts  5.83 us (7%)
  other arithmetic  3.53 us (4%)
    pallas_call x1, Pallas kernels, on_device(): pl.pallas_call(functools.partial(kernel, n, nt, ng), out_shape=jax.ShapeD...  70.6 us
    unnamed x26, local copies, waits for them, and re-layouts  5.4 us

profile of v2, /device:TPU:0, one launch (start us, length us, event | category | flops | bytes accessed | tf_op | source)
XLA Modules:
  0.0 80.1 jit_solution(15240553391106896325)
XLA Ops:
  0.0 0.7 copy-done.11
  0.7 1.0 %broadcast_select_fusion = (f32[2,128,128]{2,1,0:T(8,128)S(1)}, f32[2,128,128]{2,1,0:T(8,128)S(1)}) fusion(pred[128]{0:T(512)(128)(4,1)S(1)} %copy-done.11, f32[2,8,16,128]{3,2,1,0:T(8,128)} %param.26, f32[2,8,16,128]{3,2,1,0:T(8,128)} %param.25), kind=kLoop, calls=%fused_computation.14 | loop fusion | flops 65536 | bytes 524416 | tf_op jit(solution)/shard_map/jit(_pad)/pad | solution.py:419
  1.7 0.0 copy-done.2
  1.7 0.0 copy-start.3
  1.7 0.1 fusion.5
  1.8 0.8 copy-done.3
  2.6 0.1 fusion.6
  2.7 0.8 %copy-done = f32[2,8,16,128]{3,2,1,0:T(8,128)S(1)} copy-done((f32[2,8,16,128]{3,2,1,0:T(8,128)S(1)}, f32[2,8,16,128]{3,2,1,0:T(8,128)}, u32[]{:S(2)}) %copy-start) | copy-done | bytes 131096
  3.5 0.1 slice.28
  3.6 0.8 %copy-done.1 = f32[2,8,16,128]{3,2,1,0:T(8,128)S(1)} copy-done((f32[2,8,16,128]{3,2,1,0:T(8,128)S(1)}, f32[2,8,16,128]{3,2,1,0:T(8,128)}, u32[]{:S(2)}) %copy-start.1) | copy-done | bytes 131096
  4.4 0.1 slice.31
  4.5 0.0 copy-start.7
  4.5 0.0 copy-start.8
  4.5 0.0 copy-start.9
  4.5 0.0 copy-start.10
  4.6 1.2 %fusion = (f32[2,256,256]{2,1,0:T(8,128)}, f32[2,256,256]{2,1,0:T(8,128)}) fusion(f32[2,128,32]{2,1,0:T(8,128)S(1)} %get-tuple-element.6, f32[2,128,32]{2,1,0:T(8,128)S(1)} %get-tuple-element.5, f32[2,128,64]{2,1,0:T(8,128)S(1)} %slice.31, f32[2,128,128]{2,1,0:T(8,128)S(1)} %get-tuple-element.9, f32[2,128,32]{2,1,0:T(8,128)S(1)} %get-tuple-element.8, ...), kind=kLoop, calls=%fused_computation.1 | loop fusion | flops 3276800 | bytes 1572864 | tf_op jit(solution)/shard_map/concatenate | solution.py:423
  5.7 0.1 pad.49.clone
  5.8 0.0 copy-done.7
  5.8 0.0 copy-done.8
  5.8 0.0 copy-done.9
  5.8 0.0 copy-done.10
  5.8 0.0 copy-start.5
  5.8 0.0 copy-start.6
  5.9 0.1 maximum_bitcast_fusion
  5.9 0.6 pad_maximum_fusion.1.rt_ref
  6.5 0.1 copy-done.5
  6.6 0.0 copy-done.6
  6.6 0.6 pad_maximum_fusion.x_ref
  7.3 0.1 copy-done.4
  7.4 0.6 copy.21.taps_ref
  8.0 70.6 %shard_map.190 = bf16[128,256]{1,0:T(8,128)(2,1)} custom-call(f32[128]{0:T(128)} %spacing.1, bf16[128,256]{1,0:T(8,128)(2,1)} %pad_maximum_fusion.x_ref, f32[2,2,8,128]{3,2,1,0:T(8,128)} %pad_maximum_fusion.1.rt_ref, f32[2,256,256]{2,1,0:T(8,128)} %get-tuple-element.14.drive_ref, f32[2,256,256]{2,1,0:T(8,128)} %get-tuple-element.13.read_ref, ...), custom_call_target="tpu_custom_call" | custom-call | tf_op jit(solution)/shard_map/pallas_call | solution.py:456
  78.6 1.5 %copy.23 = bf16[128,256]{1,0:T(8,128)(2,1)} copy(bf16[128,256]{1,0:T(8,128)(2,1)} %shard_map.190) | data formatting | bytes 131072
  (6 shorter events, 0.0 us)
Async XLA Ops:
  0.0 0.7 copy-start.11
  0.7 1.0 %copy-start.2 = (f32[2,8,16,64]{3,2,1,0:T(8,128)S(1)}, f32[2,8,16,64]{3,2,1,0:T(8,128)}, u32[]{:S(2)}) copy-start(f32[2,8,16,64]{3,2,1,0:T(8,128)} %param.30) | copy-start | bytes 196612
  1.7 0.9 %copy-start.3 = (f32[2,8,16,64]{3,2,1,0:T(8,128)S(1)}, f32[2,8,16,64]{3,2,1,0:T(8,128)}, u32[]{:S(2)}) copy-start(f32[2,8,16,64]{3,2,1,0:T(8,128)} %param.29) | copy-start | bytes 196612
  2.6 0.9 %copy-start = (f32[2,8,16,128]{3,2,1,0:T(8,128)S(1)}, f32[2,8,16,128]{3,2,1,0:T(8,128)}, u32[]{:S(2)}) copy-start(f32[2,8,16,128]{3,2,1,0:T(8,128)} %param.25) | copy-start | bytes 393220
  3.5 0.9 %copy-start.1 = (f32[2,8,16,128]{3,2,1,0:T(8,128)S(1)}, f32[2,8,16,128]{3,2,1,0:T(8,128)}, u32[]{:S(2)}) copy-start(f32[2,8,16,128]{3,2,1,0:T(8,128)} %param.26) | copy-start | bytes 393220
  4.5 1.3 %copy-start.7 = (f32[2,8,32]{2,1,0:T(8,128)S(1)}, f32[2,8,32]{2,1,0:T(8,128)}, u32[]{:S(2)}) copy-start(f32[2,8,32]{2,1,0:T(8,128)} %param.27) | copy-start | bytes 6148
  4.5 1.3 %copy-start.8 = (f32[2,8,64]{2,1,0:T(8,128)S(1)}, f32[2,8,64]{2,1,0:T(8,128)}, u32[]{:S(2)}) copy-start(f32[2,8,64]{2,1,0:T(8,128)} %param.23) | copy-start | bytes 12292
  4.5 1.3 %copy-start.9 = (f32[2,8,32]{2,1,0:T(8,128)S(1)}, f32[2,8,32]{2,1,0:T(8,128)}, u32[]{:S(2)}) copy-start(f32[2,8,32]{2,1,0:T(8,128)} %param.28) | copy-start | bytes 6148
  4.5 1.3 %copy-start.10 = (f32[2,8,64]{2,1,0:T(8,128)S(1)}, f32[2,8,64]{2,1,0:T(8,128)}, u32[]{:S(2)}) copy-start(f32[2,8,64]{2,1,0:T(8,128)} %param.24) | copy-start | bytes 12292
  5.8 0.8 copy-start.5
  5.8 0.8 copy-start.6
  6.6 0.8 copy-start.4

commit v3 on v2

--- a/solution.py
+++ b/solution.py
@@ -54,9 +54,25 @@
     return lax.dot_general(a, b, (((1,), (1,)), ((), ())), preferred_element_type=f32)
 
 
+def packed(wide, narrow):
+    wide = wide.reshape(-1, wide.shape[-1])
+    narrow = narrow.reshape(-1, narrow.shape[-1])
+    states, small = wide.shape[1] // 2, narrow.shape[1] // 2
+
+    def zeros(like, lanes):
+        return jnp.zeros((like.shape[0], lanes), f32)
+
+    top = jnp.concatenate(
+        [wide[:, :states], zeros(wide, LANES - states), wide[:, states:], zeros(wide, LANES - states)], axis=1)
+    low = jnp.concatenate(
+        [zeros(narrow, states), narrow[:, :small], zeros(narrow, LANES - small),
+         narrow[:, small:], zeros(narrow, LANES - states - small)], axis=1)
+    return jnp.concatenate([top, low], axis=0)
+
+
 def kernel(
     n, nt, ng,
-    spacing, x_ref, rt_ref, drive_ref, read_ref, skip_ref, ov_ref, og_ref, stream_ref, gain_ref,
+    spacing, xw_ref, xn_ref, rw_ref, tw_ref, rn_ref, tn_ref, dw_ref, dn_ref, rdw_ref, rdn_ref, skip_ref, ov_ref, og_ref, stream_ref, gain_ref,
     taps_ref, upv_ref, upg_ref, down_ref,
     out_ref,
     upv, upg, down, kick, dec, ends, mix, mid, gain, pre, part, near, got, own, sums, done,
@@ -66,9 +82,8 @@
     me, mt, mg = lax.axis_index("sp"), lax.axis_index("tp"), lax.axis_index("grp")
     partner = mt + 1 - 2 * lax.rem(mt, 2)
     side = nt // 2
-    tokens = x_ref.shape[0]
-    groups = rt_ref.shape[2]
-    channels = x_ref.shape[1] // 2
+    tokens, channels = xw_ref.shape
+    groups = rw_ref.shape[1]
     width = upv.shape[1]
     rows = upv_ref.shape[0]
     cols = out_ref.shape[1]
@@ -149,10 +164,11 @@
         gain_copy(lax.rem(mt + offset, nt), mt).start()
     gain[mt] = gain_ref[...]
 
-    x = x_ref[...]
+    x = jnp.concatenate([xw_ref[...], xn_ref[...]], axis=1)
+    rest = jnp.ones((groups, LANES - rw_ref.shape[2] - rn_ref.shape[2]), f32)
     lane_group = lax.rem(lax.broadcasted_iota(jnp.int32, x.shape, 1), channels) // GROUP
     for d in range(2):
-        high, low = split(drive_ref[d])
+        high, low = split(packed(dw_ref[d], dn_ref[d]))
         for g in range(groups):
             picked = jnp.where(lane_group == g, x, jnp.zeros_like(x))
             pushed = dot(picked, high) + dot(picked, low)
@@ -160,8 +176,8 @@
             kick[d, 0, place, :] = pushed[:, :LANES]
             kick[d, 1, place, :] = pushed[:, LANES:]
 
-    rates = [rt_ref[0, d] for d in range(2)]
-    turns = [rt_ref[1, d] for d in range(2)]
+    rates = [jnp.concatenate([rw_ref[d], rn_ref[d], rest], axis=1) for d in range(2)]
+    turns = [jnp.concatenate([tw_ref[d], tn_ref[d], rest], axis=1) for d in range(2)]
     inverse = []
     for d in range(2):
         square = rates[d] * rates[d] + turns[d] * turns[d]
@@ -204,6 +220,7 @@
     for offset in range(1, n):
         ends_copy(lax.rem(me + offset, n), me).start()
     weight_start(1)
+    weight_start(2)
     for offset in range(1, n):
         peer = lax.rem(me + offset, n)
         ends_copy(peer, me).wait_send()
@@ -237,9 +254,9 @@
 
     lax.fori_loop(0, tokens, second, tuple(carry), unroll=4)
 
-    reading = skip_ref[...] * x.astype(f32)
+    reading = jnp.concatenate([skip_ref[0:1, :], skip_ref[1:2, :]], axis=1) * x.astype(f32)
     for d in range(2):
-        high, low = split(read_ref[d])
+        high, low = split(packed(rdw_ref[d], rdn_ref[d]))
         for g in range(groups):
             place = pl.ds(g, tokens, stride=groups)
             state = jnp.concatenate([kick[d, 0, place, :], kick[d, 1, place, :]], axis=1)
@@ -293,27 +310,18 @@
     for offset in range(1, n):
         z_copy(lax.rem(me + offset, n), me).start()
     spread(me)
-    weight_start(2)
-    for offset in range(1, n):
-        peer = lax.rem(me + offset, n)
-        z_copy(me, peer).wait_recv()
-        spread(peer)
-        relay(lax.rem(me + offset - 1, n))
-    relay(lax.rem(me + n - 1, n))
     for offset in range(1, nt):
         peer = lax.rem(mt + offset, nt)
         gain_copy(peer, mt).wait_send()
         gain_copy(mt, peer).wait_recv()
+    for i in range(2):
+        pre[pl.ds(i * (8 + n * tokens), 8), :] = jnp.zeros((8, 2 * width), f32)
+    weight_share(2)
+    relay(me)
     weight_wait(0)
     weight_wait(1)
-    for offset in range(1, n):
-        z_copy(lax.rem(me + offset, n), me).wait_send()
-    weight_share(2)
-
-    for i in range(2):
-        pre[pl.ds(i * (8 + n * tokens), 8), :] = jnp.zeros((8, 2 * width), f32)
-    for step in range(n):
-        s = lax.rem(me + step, n)
+
+    def raise_block(s):
         for offset in range(side):
             peer = lax.rem(mt + 2 * offset, nt)
             if offset:
@@ -330,6 +338,16 @@
         place = pl.ds(pl.multiple_of(8 + s * tokens, 8), tokens)
         pre[place, :width] = dot(normed, upv[...]).astype(bf16).astype(f32)
         pre[place, width:] = dot(normed, upg[...]).astype(bf16).astype(f32)
+
+    for offset in range(1, n):
+        peer = lax.rem(me + offset, n)
+        z_copy(me, peer).wait_recv()
+        spread(peer)
+        raise_block(lax.rem(me + offset - 1, n))
+        relay(peer)
+    raise_block(lax.rem(me + n - 1, n))
+    for offset in range(1, n):
+        z_copy(lax.rem(me + offset, n), me).wait_send()
 
     weight_wait(2)
     begin = start_of(me)
@@ -406,23 +424,6 @@
     out_ref[...] = (mid[me, mt].astype(f32) + total).astype(bf16)
 
 
-def packed(wide, narrow):
-    def halves(value):
-        states = value.shape[3] // 2
-        flat = value.reshape(2, -1, 2 * states)
-        return flat[..., :states], flat[..., states:]
-
-    wide_parts, narrow_parts = halves(wide), halves(narrow)
-    count, states = wide_parts[0].shape[1:]
-    small = narrow_parts[0].shape[2]
-    top = jnp.concatenate(
-        [jnp.pad(part, ((0, 0), (0, 0), (0, LANES - states))) for part in wide_parts], axis=2)
-    low = jnp.concatenate(
-        [jnp.pad(part, ((0, 0), (0, 0), (states, LANES - states - small))) for part in narrow_parts],
-        axis=2)
-    return jnp.concatenate([top, low], axis=1)
-
-
 def on_device(
     n, nt, ng,
     input_wide, input_narrow, spacing, rate_wide, turn_wide, drive_wide, read_wide,
@@ -431,14 +432,6 @@
 ):
     tokens = spacing.shape[0]
     groups = rate_wide.shape[1]
-    x = jnp.concatenate([input_wide, input_narrow], axis=1)
-    rest = LANES - rate_wide.shape[2] - narrow_decay_rate.shape[2]
-    ones = jnp.ones((2, groups, rest), f32)
-    rt = jnp.stack([jnp.concatenate([rate_wide, narrow_decay_rate, ones], axis=2),
-                    jnp.concatenate([turn_wide, turn_narrow, ones], axis=2)])
-    drive = packed(drive_wide, drive_narrow)
-    read = packed(read_wide, read_narrow)
-    skip = skip_gain.reshape(1, -1)
     extra = -up_value.shape[1] % LANES
     if extra:
         up_value = jnp.pad(up_value, ((0, 0), (0, extra)))
@@ -456,7 +449,7 @@
     return pl.pallas_call(
         functools.partial(kernel, n, nt, ng),
         out_shape=jax.ShapeDtypeStruct((tokens, cols), bf16),
-        in_specs=[pl.BlockSpec(memory_space=pltpu.SMEM)] + [vmem] * 10 + [anywhere] * 3,
+        in_specs=[pl.BlockSpec(memory_space=pltpu.SMEM)] + [vmem] * 16 + [anywhere] * 3,
         out_specs=vmem,
         scratch_shapes=[
             pltpu.VMEM((rows * n, width), bf16),
@@ -465,7 +458,7 @@
             pltpu.VMEM((2, 2, tokens * groups, LANES), f32),
             pltpu.VMEM((2, 2, tokens * groups, LANES), f32),
             pltpu.VMEM((n, 2, 4, groups, LANES), f32),
-            pltpu.VMEM((nt, tokens, x.shape[1]), bf16),
+            pltpu.VMEM((nt, tokens, 2 * input_wide.shape[1]), bf16),
             pltpu.VMEM((n, nt, tokens, cols), bf16),
             pltpu.VMEM((nt, 1, cols), f32),
             pltpu.VMEM((n * tokens + 16, 2 * width), f32),
@@ -487,7 +480,8 @@
         ],
         compiler_params=pltpu.CompilerParams(
             collective_id=0, has_side_effects=True, vmem_limit_bytes=60 * 1024 * 1024),
-    )(spacing, x, rt, drive, read, skip, out_value, out_gate, stream, norm_gain.reshape(1, -1),
+    )(spacing, input_wide, input_narrow, rate_wide, turn_wide, narrow_decay_rate, turn_narrow,
+      drive_wide, drive_narrow, read_wide, read_narrow, skip_gain, out_value, out_gate, stream, norm_gain.reshape(1, -1),
       conv_taps, up_value, up_gate, down_weight)
 
 

time: 80.5 us -> 73 us (0.907)
  other arithmetic: 3.53 us -> 0 us
  local copies, waits for them, and re-layouts: 5.83 us -> 2.86 us
    unnamed x26 -> x2, local copies, waits for them, and re-layouts: 5.4 us -> 2.86 us
    concatenate x2 -> x0, other arithmetic: 1.82 us -> none  [the longest x1 1.18 us: packed(): return jnp.concatenate([top, low], axis=1)]
    pad x1 -> x0, other arithmetic: 1.02 us -> none  [packed(): jnp.pad(part, ((0, 0), (0, 0), (0, LANES - states)))]
where the time goes in v3:
time: 73 us; the launch traced here: 72.8 us
  Pallas kernels  69.9 us (96%)
  local copies, waits for them, and re-layouts  2.86 us (4%)
    pallas_call x1, Pallas kernels, on_device(): pl.pallas_call(functools.partial(kernel, n, nt, ng), out_shape=jax.ShapeD...  69.9 us
    unnamed x2, local copies, waits for them, and re-layouts  2.86 us

profile of v3, /device:TPU:0, one launch (start us, length us, event | category | flops | bytes accessed | tf_op | source)
XLA Modules:
  0.0 72.8 jit_solution(10221748202442440785)
XLA Ops:
  0.0 1.4 %copy.21.taps_ref = f32[2,3,1408]{2,1,0:T(4,128)} copy(f32[2,3,1408]{2,0,1:T(2,128)} %param.38) | data formatting | bytes 67584 | tf_op args[18]
  1.4 69.9 %shard_map.190 = bf16[128,256]{1,0:T(8,128)(2,1)} custom-call(f32[128]{0:T(128)} %spacing.1, bf16[128,128]{1,0:T(8,128)(2,1)} %xw_ref.1, bf16[128,128]{1,0:T(8,128)(2,1)} %xn_ref.1, f32[2,8,64]{2,1,0:T(8,128)} %rw_ref.1, f32[2,8,64]{2,1,0:T(8,128)} %tw_ref.1, f32[2,8,32]{2,1,0:T(8,128)} %rn_ref.1, f32[2,8,32]{2,1,0:T(8,128)} %tn_ref.1, ...), custom_call_target="tpu_custom_call" | custom-call | tf_op jit(solution)/shard_map/pallas_call | solution.py:449
  71.3 1.5 %copy.23 = bf16[128,256]{1,0:T(8,128)(2,1)} copy(bf16[128,256]{1,0:T(8,128)(2,1)} %shard_map.190) | data formatting | bytes 131072

commit v4 on v3

--- a/solution.py
+++ b/solution.py
@@ -207,20 +207,18 @@
 
     zero = jnp.zeros((groups, LANES), f32)
     found = lax.fori_loop(0, tokens, first, (zero, zero, zero, zero, jnp.float32(0.0)), unroll=4)
+    last_lane = lax.broadcasted_iota(jnp.int32, zero.shape, 1) == LANES - 1
     for d in range(2):
-        ar, ai = decay_of(rates[d], turns[d], found[4])
-        ends[me, d, 0] = found[2 * d]
+        ends[me, d, 0] = jnp.where(last_lane, found[4], found[2 * d])
         ends[me, d, 1] = found[2 * d + 1]
-        ends[me, d, 2] = ar
-        ends[me, d, 3] = ai
 
     def ends_copy(target, slot):
-        return remote(ends.at[slot], ends.at[slot], e_send.at[target], e_recv.at[slot], "sp", target)
+        d = jnp.where(target > slot, 0, 1)
+        return remote(ends.at[slot, d], ends.at[slot, d], e_send.at[target], e_recv.at[slot], "sp", target)
 
     for offset in range(1, n):
         ends_copy(lax.rem(me + offset, n), me).start()
     weight_start(1)
-    weight_start(2)
     for offset in range(1, n):
         peer = lax.rem(me + offset, n)
         ends_copy(peer, me).wait_send()
@@ -232,7 +230,7 @@
         for k in range(n):
             s = k if d == 0 else n - 1 - k
             use = (s < me) if d == 0 else (s > me)
-            nr, ni = times(ends[s, d, 2], ends[s, d, 3], cr, ci)
+            nr, ni = times(*decay_of(rates[d], turns[d], ends[s, d, 0][:, LANES - 1:]), cr, ci)
             flag = jnp.where(use, 1, 0)
             keep = jnp.full((groups, LANES), flag, jnp.int32) == 1
             cr = jnp.where(keep, nr + ends[s, d, 0], cr)
@@ -270,6 +268,7 @@
 
     for offset in range(1, nt):
         mix_copy(lax.rem(mt + offset, nt), mt).start()
+    weight_start(2)
     for offset in range(1, nt):
         peer = lax.rem(mt + offset, nt)
         mix_copy(peer, mt).wait_send()
@@ -457,7 +456,7 @@
             pltpu.VMEM((n, width, per), bf16),
             pltpu.VMEM((2, 2, tokens * groups, LANES), f32),
             pltpu.VMEM((2, 2, tokens * groups, LANES), f32),
-            pltpu.VMEM((n, 2, 4, groups, LANES), f32),
+            pltpu.VMEM((n, 2, 2, groups, LANES), f32),
             pltpu.VMEM((nt, tokens, 2 * input_wide.shape[1]), bf16),
             pltpu.VMEM((n, nt, tokens, cols), bf16),
             pltpu.VMEM((nt, 1, cols), f32),

time: 73 us -> 68.7 us (0.941)
  Pallas kernels: 69.9 us -> 65.5 us
    pallas_call x1, Pallas kernels: 69.9 us -> 65.5 us  [on_device(): pl.pallas_call(functools.partial(kernel, n, nt, ng), out_shape=jax.ShapeD...]
where the time goes in v4:
time: 68.7 us; the launch traced here: 68.4 us
  Pallas kernels  65.5 us (95%)
  local copies, waits for them, and re-layouts  2.86 us (4%)
    pallas_call x1, Pallas kernels, on_device(): pl.pallas_call(functools.partial(kernel, n, nt, ng), out_shape=jax.ShapeD...  65.5 us
    unnamed x2, local copies, waits for them, and re-layouts  2.86 us

profile of v4, /device:TPU:0, one launch (start us, length us, event | category | flops | bytes accessed | tf_op | source)
XLA Modules:
  0.0 68.4 jit_solution(12390321475016380325)
XLA Ops:
  0.0 1.4 %copy.21.taps_ref = f32[2,3,1408]{2,1,0:T(4,128)} copy(f32[2,3,1408]{2,0,1:T(2,128)} %param.38) | data formatting | bytes 67584 | tf_op args[18]
  1.4 65.5 %shard_map.190 = bf16[128,256]{1,0:T(8,128)(2,1)} custom-call(f32[128]{0:T(128)} %spacing.1, bf16[128,128]{1,0:T(8,128)(2,1)} %xw_ref.1, bf16[128,128]{1,0:T(8,128)(2,1)} %xn_ref.1, f32[2,8,64]{2,1,0:T(8,128)} %rw_ref.1, f32[2,8,64]{2,1,0:T(8,128)} %tw_ref.1, f32[2,8,32]{2,1,0:T(8,128)} %rn_ref.1, f32[2,8,32]{2,1,0:T(8,128)} %tn_ref.1, ...), custom_call_target="tpu_custom_call" | custom-call | tf_op jit(solution)/shard_map/pallas_call | solution.py:448
  66.9 1.5 %copy.23 = bf16[128,256]{1,0:T(8,128)(2,1)} copy(bf16[128,256]{1,0:T(8,128)(2,1)} %shard_map.190) | data formatting | bytes 131072
